TPU v7x, 32 devices: a whole 2x2x4 slice. The times are simulated.
32 devices in a mesh: ep: 16 (over z, y, x), tp: 2 (over core).
Axes of the slice: x: 2, y: 2, z: 4, core: 2. Of those that a mesh axis runs over, the one named last changes fastest.
Arguments:
- tokens: bfloat16 [256, 2048], P('ep'), may hold values from -6 to 6
- lengths: int32 [256], P('ep'), may hold values from 1 to 1024, as said below
- attn_gain: float32 [2048], replicated, may hold values from 0.1 to 1.9
- w_query: bfloat16 [2048, 1024], P(None, 'tp'), may hold values from -0.125 to 0.125
- w_key: bfloat16 [2048, 128], P(None, 'tp'), may hold values from -0.125 to 0.125
- w_value: bfloat16 [2048, 128], P(None, 'tp'), may hold values from -0.125 to 0.125
- head_bias: float32 [16], P('tp'), may hold values from -7 to -2
- key_cache: bfloat16 [256, 2, 64, 1024], P('ep', 'tp'), may hold values from -6 to 6
- value_cache: bfloat16 [256, 2, 64, 1024], P('ep', 'tp'), may hold values from -6 to 6
- w_attn_out: bfloat16 [1024, 2048], P('tp'), may hold values from -0.1875 to 0.1875
- ffn_gain: float32 [2048], replicated, may hold values from 0.1 to 1.9
- w_router: bfloat16 [2048, 16], replicated, may hold values from -0.125 to 0.125
- routes: int32 [256, 6], P('ep'), may hold values from 0 to 15, all different within a row; in each aligned block of 16 rows (0 to 15, 16 to 31, ...) at most 12 rows name the same one
- w_dense_gate: bfloat16 [2048, 512], P('ep', 'tp'), may hold values from -0.125 to 0.125
- w_dense_up: bfloat16 [2048, 512], P('ep', 'tp'), may hold values from -0.125 to 0.125
- w_dense_down: bfloat16 [512, 2048], P('tp', 'ep'), may hold values from -0.25 to 0.25
- dense_mix: float32 [2048], replicated, may hold values from -0.125 to 0.125
- w_expert_gate: bfloat16 [16, 2048, 512], P('ep', None, 'tp'), may hold values from -0.125 to 0.125
- w_expert_up: bfloat16 [16, 2048, 512], P('ep', None, 'tp'), may hold values from -0.125 to 0.125
- w_expert_down: bfloat16 [16, 512, 2048], P('ep', 'tp'), may hold values from -0.25 to 0.25
Outputs:
- layer_out: bfloat16 [256, 2048], P('ep', 'tp')
- new_keys: bfloat16 [256, 128], P('ep', 'tp')
- new_values: bfloat16 [256, 128], P('ep', 'tp')
Inputs may be any that keep to these rules, and one draw needn't show every extreme that they name: `lengths`: every sequence holds between 1 and 1024 cached positions; in every draw some sequence holds exactly 1024. `routes`: each token names 6 different experts. Among the rows of one device no expert is named by more than 12 rows.
All inputs are finite; a program needn't handle non-finite values.
Results may differ from a plain program's by a relative error of at most 0.014.
Values may be sent and summed in bfloat16 or wider, within the bound.
A program may use at most 64 MiB of HBM per device.

v0:
```python
import jax
import jax.numpy as jnp
from jax import lax
from jax.sharding import PartitionSpec as P


def rms_scale(values, gain):
    wide = values.astype(jnp.float32)
    return wide * lax.rsqrt(jnp.mean(wide * wide, axis=-1, keepdims=True) + 1e-06) * gain


def stick_read(queries, lengths, head_bias, key_cache, value_cache):
    seq_count, local_kv, head_dim, cache_len = key_cache.shape
    group_size = head_bias.shape[0] // local_kv
    grouped = queries.reshape(seq_count, local_kv, group_size, head_dim)
    head_shift = head_bias.reshape(1, local_kv, group_size, 1)
    span_len = min(512, cache_len)
    block_count = (jnp.max(lengths) + span_len - 1) // span_len
    span_index = lax.iota(jnp.int32, span_len)
    after_mask = (span_index[:, None] > span_index[None, :]).astype(jnp.float32)

    def visit(visit_index, carry):
        totals, log_later = carry
        first = (block_count - 1 - visit_index) * span_len
        key_block = lax.dynamic_slice_in_dim(key_cache, first, span_len, 3)
        value_block = lax.dynamic_slice_in_dim(value_cache, first, span_len, 3)
        scores = (
            jnp.einsum("skgd,skdc->skgc", grouped, key_block, preferred_element_type=jnp.float32)
            * head_dim ** (-0.5)
            + head_shift
        )
        positions = first + span_index
        visible = (positions[None, :] < lengths[:, None])[:, None, None, :]
        log_keep = jnp.where(visible, jax.nn.log_sigmoid(-scores), 0.0)
        log_after = (
            jnp.einsum("skgj,jc->skgc", log_keep, after_mask, precision=lax.Precision.HIGHEST)
            + log_later[..., None]
        )
        weights = jnp.where(visible, jnp.exp(jax.nn.log_sigmoid(scores) + log_after), 0.0).astype(
            jnp.bfloat16
        )
        totals = totals + jnp.einsum(
            "skgc,skdc->skgd", weights, value_block, preferred_element_type=jnp.float32
        )
        return (totals, log_later + jnp.sum(log_keep, axis=3))

    start_totals = jnp.zeros((seq_count, local_kv, group_size, head_dim), jnp.float32)
    start_later = jnp.zeros((seq_count, local_kv, group_size), jnp.float32)
    totals, unused_later = lax.fori_loop(0, block_count, visit, (start_totals, start_later))
    return totals.reshape(seq_count, -1).astype(jnp.bfloat16)


def expert_math(inputs, w_expert_gate, w_expert_up, w_expert_down):
    gate_rows = jnp.einsum(
        "njcd,jdf->njcf", inputs, w_expert_gate, preferred_element_type=jnp.float32
    )
    up_rows = jnp.einsum("njcd,jdf->njcf", inputs, w_expert_up, preferred_element_type=jnp.float32)
    hidden = (jax.nn.silu(gate_rows) * up_rows).astype(jnp.bfloat16)
    partial_value = jnp.einsum(
        "njcf,jfd->njcd", hidden, w_expert_down, preferred_element_type=jnp.float32
    ).astype(jnp.bfloat16)
    return (
        lax.psum_scatter(partial_value, "tp", scatter_dimension=3, tiled=True)
        .astype(jnp.float32)
        .astype(jnp.bfloat16)
    )


def shards(
    tokens,
    lengths,
    attn_gain,
    w_query,
    w_key,
    w_value,
    head_bias,
    key_cache,
    value_cache,
    w_attn_out,
    ffn_gain,
    w_router,
    routes,
    w_dense_gate,
    w_dense_up,
    w_dense_down,
    dense_mix,
    w_expert_gate,
    w_expert_up,
    w_expert_down,
):
    seq_count, model_width = tokens.shape
    normed = rms_scale(tokens, attn_gain).astype(jnp.bfloat16)
    new_keys = jnp.dot(normed, w_key, preferred_element_type=jnp.float32).astype(jnp.bfloat16)
    new_values = jnp.dot(normed, w_value, preferred_element_type=jnp.float32).astype(jnp.bfloat16)
    queries = jnp.dot(normed, w_query, preferred_element_type=jnp.float32).astype(jnp.bfloat16)
    heads_out = stick_read(queries, lengths, head_bias, key_cache, value_cache)
    attn_partial = jnp.dot(heads_out, w_attn_out, preferred_element_type=jnp.float32).astype(
        jnp.bfloat16
    )
    attn = lax.psum(attn_partial, "tp").astype(jnp.float32)
    residual = (tokens.astype(jnp.float32) + attn).astype(jnp.bfloat16)
    normed2 = rms_scale(residual, ffn_gain).astype(jnp.bfloat16)
    expert_total = w_router.shape[1]
    top_count = routes.shape[1]
    probs = jax.nn.sigmoid(jnp.dot(normed2, w_router, preferred_element_type=jnp.float32))
    hits = routes[:, :, None] == lax.iota(jnp.int32, expert_total)[None, None, :]
    picked = jnp.sum(jnp.where(hits, probs[:, None, :], 0.0), axis=-1)
    gates = picked / jnp.sum(picked, axis=-1, keepdims=True) * 2.5
    capacity = max(2, 2 * seq_count * top_count // expert_total)
    slot_total = expert_total * capacity
    flat_routes = routes.reshape(-1)
    route_count = flat_routes.shape[0]
    matching = flat_routes[:, None] == flat_routes[None, :]
    earlier = lax.iota(jnp.int32, route_count)[:, None] > lax.iota(jnp.int32, route_count)[None, :]
    slot_rank = jnp.sum(jnp.logical_and(matching, earlier).astype(jnp.int32), axis=1)
    target = flat_routes * capacity + slot_rank
    one_hot = (target[:, None] == lax.iota(jnp.int32, slot_total)[None, :]).astype(jnp.bfloat16)
    dispatch = jnp.sum(one_hot.reshape(seq_count, top_count, slot_total), axis=1)
    send_rows = jnp.einsum(
        "sr,sd->rd", dispatch, normed2, preferred_element_type=jnp.float32
    ).astype(jnp.bfloat16)
    send_rows = send_rows.reshape(expert_total, capacity, model_width)
    local_experts = w_expert_gate.shape[0]
    received = lax.all_to_all(send_rows, "ep", split_axis=0, concat_axis=0, tiled=True)
    source_count = received.shape[0] // local_experts
    item_count = received.shape[1]
    inputs = received.reshape(source_count, local_experts, item_count, model_width)
    summed = expert_math(inputs, w_expert_gate, w_expert_up, w_expert_down)
    summed = summed.reshape(source_count * local_experts, item_count, summed.shape[3])
    returned = lax.all_to_all(summed, "ep", split_axis=0, concat_axis=0, tiled=True)
    half_width = returned.shape[2]
    route_rows = returned.reshape(slot_total, half_width)[target]
    route_rows = route_rows.reshape(seq_count, top_count, half_width)
    routed = jnp.sum(gates[:, :, None] * route_rows.astype(jnp.float32), axis=1)
    features2 = lax.all_to_all(normed2, "ep", split_axis=1, concat_axis=0, tiled=True)
    paired_weights = jnp.concatenate([w_dense_gate, w_dense_up], axis=1)
    paired = lax.psum_scatter(
        jnp.dot(features2, paired_weights, preferred_element_type=jnp.float32),
        "ep",
        scatter_dimension=0,
        tiled=True,
    )
    hidden_cols = w_dense_gate.shape[1]
    dense_gate_rows = paired[:, :hidden_cols]
    dense_up_rows = paired[:, hidden_cols:]
    dense_hidden = (jax.nn.silu(dense_gate_rows) * dense_up_rows).astype(jnp.bfloat16)
    dense_columns = jnp.dot(
        lax.all_gather(dense_hidden, "ep", axis=0, tiled=True),
        w_dense_down,
        preferred_element_type=jnp.float32,
    )
    dense_partial = lax.all_to_all(
        dense_columns.astype(jnp.bfloat16), "ep", split_axis=0, concat_axis=1, tiled=True
    )
    dense = lax.psum_scatter(dense_partial, "tp", scatter_dimension=1, tiled=True).astype(
        jnp.float32
    )
    mix_gate = jax.nn.sigmoid(jnp.sum(normed2.astype(jnp.float32) * dense_mix, axis=-1))
    offset = lax.axis_index("tp") * half_width
    residual_half = lax.dynamic_slice_in_dim(residual, offset, half_width, 1)
    layer_out = (residual_half.astype(jnp.float32) + mix_gate[:, None] * dense + routed).astype(
        jnp.bfloat16
    )
    return (layer_out, new_keys, new_values)


def solution(mesh):
    return jax.shard_map(
        shards,
        mesh=mesh,
        in_specs=(
            P("ep", None),
            P("ep"),
            P(),
            P(None, "tp"),
            P(None, "tp"),
            P(None, "tp"),
            P("tp"),
            P("ep", "tp", None, None),
            P("ep", "tp", None, None),
            P("tp", None),
            P(),
            P(),
            P("ep", None),
            P("ep", "tp"),
            P("ep", "tp"),
            P("tp", "ep"),
            P(),
            P("ep", None, "tp"),
            P("ep", None, "tp"),
            P("ep", "tp", None),
        ),
        out_specs=(P("ep", "tp"), P("ep", "tp"), P("ep", "tp")),
        check_vma=False,
    )
```

profile of v0, /device:TPU:0, one launch (start us, length us, event | category | flops | bytes accessed | tf_op | source)
XLA Modules:
  0.0 217.0 jit_solution(16179048854171437925)
XLA Ops:
  7.2 1.4 reduce_max.9
  9.3 1.0 fusion.40
  10.3 2.1 convolution_convert_fusion.4
  12.5 3.9 %while.15 = (s32[]{:T(128)}, f32[16,1,8,64]{3,2,0,1:T(8,128)S(1)}, f32[16,1,8]{0,2,1:T(8,128)S(1)}, s32[]{:T(128)}, s32[]{:T(128)}, /*index=5*/s32[16]{0:T(128)S...) while((s32[]{:T(128)}, f32[16,1,8,64]{3,2,0,1:T(8,128)S(1)}, ...), condition=%wide.region_4.5_spmd.clone, body=%wide.region_2.4_spmd.clone.sunk | while | flops 422003200 | bytes 11420487 | solution.py:49
  12.7 1.6 fusion.88
  14.4 0.9 fusion.89
  15.3 0.7 copy-done.1
  16.6 1.0 convolution_convert_fusion.2
  18.3 23.8 %all-reduce.2.cloned.1.call-done = bf16[16,2048]{1,0:T(8,128)(2,1)} async-done(((bf16[16,2048]{1,0:T(8,128)(2,1)}), bf16[16,2048]{1,0:T(8,128)(2,1)}) %all-reduce.2.cloned.1.call-update) | async-done | bytes 65552 | tf_op jit(solution)/shard_map/psum | solution.py:100
  42.1 1.0 fusion.37
  43.9 6.8 %all-to-all-start = ((bf16[16,16,128]{2,0,1:T(8,128)(2,1)}), bf16[16,16,128]{2,0,1:T(8,128)(2,1)S(1)}, u32[]{:S(2)}, u32[]{:S(2)}) async-start(bf16[16,16,128]{2,0,1:T(8,128)(2,1)} %bitcast.105), calls=%async_computation | async-start | bytes 131072 | tf_op jit(solution)/shard_map/all_to_all | solution.py:135
  51.2 1.2 reshape.240
  52.3 5.9 %all-to-all-done = bf16[16,16,128]{2,0,1:T(8,128)(2,1)S(1)} async-done(((bf16[16,16,128]{2,0,1:T(8,128)(2,1)}), bf16[16,16,128]{2,0,1:T(8,128)(2,1)S(1)}, u32[]{:S(2)}, u32[]{:S(2)}) %all-to-all-start) | async-done | bytes 65568 | tf_op jit(solution)/shard_map/all_to_all | solution.py:135
  58.3 3.7 %all-to-all-start.2 = ((bf16[16,12,2048]{2,1,0:T(8,128)(2,1)}), bf16[16,12,2048]{2,1,0:T(8,128)(2,1)S(1)}, u32[]{:S(2)}, u32[]{:S(2)}) async-start(bf16[16,12,2048]{2,1,0:T(8,128)(2,1)} %reshape.240), calls=%async_computation.4 | async-start | bytes 2097152 | tf_op jit(solution)/shard_map/all_to_all | solution.py:124
  62.0 1.0 fusion.44
  63.2 23.2 %all-to-all-done.2 = bf16[16,12,2048]{2,1,0:T(8,128)(2,1)S(1)} async-done(((bf16[16,12,2048]{2,1,0:T(8,128)(2,1)}), bf16[16,12,2048]{2,1,0:T(8,128)(2,1)S(1)}, u32[]{:S(2)}, u32[]{:S(2)}) %all-to-all-start.2) | async-done | bytes 786464 | tf_op jit(solution)/shard_map/all_to_all | solution.py:124
  86.4 1.7 convolution_bitcast_fusion.2
  88.7 0.8 copy-done.2
  89.5 1.3 fusion.27
  90.8 0.8 convolution_convert_fusion.5
  91.6 0.8 convolution_convert_fusion.6
  92.5 51.5 %reduce-scatter.4.cloned.1.call-done = f32[16,512]{1,0:T(8,128)} async-done(((f32[256,512]{1,0:T(8,128)}), f32[16,512]{1,0:T(8,128)}) %reduce-scatter.4.cloned.1.call-update) | async-done | bytes 32784 | tf_op jit(solution)/shard_map/reduce_scatter | solution.py:137
  144.0 0.7 fusion.52
  144.7 37.0 %all_gather.3 = bf16[256,256]{1,0:T(8,128)(2,1)S(1)} all-gather(bf16[16,256]{1,0:T(8,128)(2,1)S(1)} %fusion.52), channel_id=1, replica_groups=mesh['ep'=16,'tp'=2] {'ep'}, dimensions={0}, use_global_device_ids=true | all-gather | bytes 139264 | tf_op jit(solution)/shard_map/all_gather | solution.py:148
  181.7 0.8 convolution_convert_fusion.3
  182.5 3.5 %all-to-all-start.1 = ((bf16[16,16,128]{2,1,0:T(8,128)(2,1)}), bf16[16,16,128]{2,1,0:T(8,128)(2,1)S(1)}, u32[]{:S(2)}, u32[]{:S(2)}) async-start(bf16[16,16,128]{2,1,0:T(8,128)(2,1)} %bitcast.5), calls=%async_computation.2 | async-start | bytes 131072 | tf_op jit(solution)/shard_map/all_to_all | solution.py:152
  186.5 2.0 copy.64
  188.5 5.0 %all-to-all-done.1 = bf16[16,16,128]{2,1,0:T(8,128)(2,1)S(1)} async-done(((bf16[16,16,128]{2,1,0:T(8,128)(2,1)}), bf16[16,16,128]{2,1,0:T(8,128)(2,1)S(1)}, u32[]{:S(2)}, u32[]{:S(2)}) %all-to-all-start.1) | async-done | bytes 65568 | tf_op jit(solution)/shard_map/all_to_all | solution.py:152
  193.5 3.6 %all-to-all-start.3 = ((bf16[16,12,1024]{2,1,0:T(8,128)(2,1)}), bf16[16,12,1024]{2,1,0:T(8,128)(2,1)S(1)}, u32[]{:S(2)}, u32[]{:S(2)}) async-start(bf16[16,12,1024]{2,1,0:T(8,128)(2,1)} %copy.64), calls=%async_computation.6 | async-start | bytes 1048576 | tf_op jit(solution)/shard_map/all_to_all | solution.py:130
  197.9 9.9 %all-to-all-done.3 = bf16[16,12,1024]{2,1,0:T(8,128)(2,1)S(1)} async-done(((bf16[16,12,1024]{2,1,0:T(8,128)(2,1)}), bf16[16,12,1024]{2,1,0:T(8,128)(2,1)S(1)}, u32[]{:S(2)}, u32[]{:S(2)}) %all-to-all-start.3) | async-done | bytes 393248 | tf_op jit(solution)/shard_map/all_to_all | solution.py:130
  207.9 0.8 gather_fusion
  209.0 1.5 add_convert_fusion
  (78 shorter events, 5.1 us)
Async XLA Ops:
  7.2 9.4 %copy-start = (bf16[512,2048]{1,0:T(8,128)(2,1)S(1)}, bf16[512,2048]{1,0:T(8,128)(2,1)}, u32[]{:S(2)}) copy-start(bf16[512,2048]{1,0:T(8,128)(2,1)} %param.31) | copy-start | bytes 6291460
  7.2 5.3 %copy-start.9 = (s32[16]{0:T(128)S(1)}, s32[16]{0:T(128)}, u32[]{:S(2)}) copy-start(s32[16]{0:T(128)} %param.23) | copy-start | bytes 196
  7.2 5.3 %copy-start.16 = (f32[8]{0:T(128)S(1)}, f32[8]{0:T(128)}, u32[]{:S(2)}) copy-start(f32[8]{0:T(128)} %param.28) | copy-start | bytes 100
  7.2 34.9 %all-reduce.2.cloned.1.call-start = ((), (), s32[]{:S(2)}) async-start(), calls=%async_computation.7 | async-start | bytes 131072 | tf_op jit(solution)/shard_map/psum | solution.py:100
  14.4 1.6 copy-start.1
  16.4 1.2 copy-start.8
  16.4 25.7 %copy-start.3 = (bf16[16,2048]{1,0:T(8,128)(2,1)S(1)}, bf16[16,2048]{1,0:T(8,128)(2,1)}, u32[]{:S(2)}) copy-start(bf16[16,2048]{1,0:T(8,128)(2,1)} %param.22) | copy-start | bytes 196612
  16.4 26.6 %copy-start.7 = (f32[2048]{0:T(1024)S(1)}, f32[2048]{0:T(1024)}, u32[]{:S(2)}) copy-start(f32[2048]{0:T(1024)} %param.32) | copy-start | bytes 24580
  16.4 26.6 %copy-start.11 = (f32[2048]{0:T(1024)S(1)}, f32[2048]{0:T(1024)}, u32[]{:S(2)}) copy-start(f32[2048]{0:T(1024)} %param.38) | copy-start | bytes 24580
  43.9 14.4 %all-to-all-start = ((bf16[16,16,128]{2,0,1:T(8,128)(2,1)}), bf16[16,16,128]{2,0,1:T(8,128)(2,1)S(1)}, u32[]{:S(2)}, u32[]{:S(2)}) async-start(bf16[16,16,128]{2,0,1:T(8,128)(2,1)} %bitcast.105), calls=%async_computation | async-start | bytes 131072 | tf_op jit(solution)/shard_map/all_to_all | solution.py:135
  51.2 10.8 %copy-start.5 = (bf16[128,256]{1,0:T(8,128)(2,1)S(1)}, bf16[128,256]{1,0:T(8,128)(2,1)}, u32[]{:S(2)}) copy-start(bf16[128,256]{1,0:T(8,128)(2,1)} %param.36) | copy-start | bytes 196612
  51.2 10.8 %copy-start.6 = (bf16[128,256]{1,0:T(8,128)(2,1)S(1)}, bf16[128,256]{1,0:T(8,128)(2,1)}, u32[]{:S(2)}) copy-start(bf16[128,256]{1,0:T(8,128)(2,1)} %param.35) | copy-start | bytes 196612
  58.3 28.1 %all-to-all-start.2 = ((bf16[16,12,2048]{2,1,0:T(8,128)(2,1)}), bf16[16,12,2048]{2,1,0:T(8,128)(2,1)S(1)}, u32[]{:S(2)}, u32[]{:S(2)}) async-start(bf16[16,12,2048]{2,1,0:T(8,128)(2,1)} %reshape.240), calls=%async_computation.4 | async-start | bytes 2097152 | tf_op jit(solution)/shard_map/all_to_all | solution.py:124
  62.0 82.0 %reduce-scatter.4.cloned.1.call-start = ((), (), s32[]{:S(2)}) async-start(), calls=%async_computation.8 | async-start | bytes 557056 | tf_op jit(solution)/shard_map/reduce_scatter | solution.py:137
  63.1 123.4 %reduce-scatter.8.cloned.1.call-start = ((), (), s32[]{:S(2)}) async-start(), calls=%async_computation.10 | async-start | bytes 1179648 | tf_op jit(solution)/shard_map/reduce_scatter | solution.py:63
  86.4 1.8 copy-start.12
  88.2 1.2 copy-start.2
  89.4 1.3 copy-start.10
  89.4 1.3 copy-start.13
  89.4 2.2 %copy-start.14 = (bf16[2048,64]{0,1:T(8,128)(2,1)S(1)}, bf16[2048,64]{0,1:T(8,128)(2,1)}, u32[]{:S(2)}) copy-start(bf16[2048,64]{0,1:T(8,128)(2,1)} %param.26) | copy-start | bytes 786436
  89.5 92.3 %copy-start.4 = (bf16[256,128]{1,0:T(8,128)(2,1)S(1)}, bf16[256,128]{1,0:T(8,128)(2,1)}, u32[]{:S(2)}) copy-start(bf16[256,128]{1,0:T(8,128)(2,1)} %param.37) | copy-start | bytes 196612
  89.5 96.5 %copy-start.15 = (bf16[2048,16]{0,1:T(8,128)(2,1)S(1)}, bf16[2048,16]{0,1:T(8,128)(2,1)}, u32[]{:S(2)}) copy-start(bf16[2048,16]{0,1:T(8,128)(2,1)} %param.33) | copy-start | bytes 196612
  182.5 11.0 %all-to-all-start.1 = ((bf16[16,16,128]{2,1,0:T(8,128)(2,1)}), bf16[16,16,128]{2,1,0:T(8,128)(2,1)S(1)}, u32[]{:S(2)}, u32[]{:S(2)}) async-start(bf16[16,16,128]{2,1,0:T(8,128)(2,1)} %bitcast.5), calls=%async_computation.2 | async-start | bytes 131072 | tf_op jit(solution)/shard_map/all_to_all | solution.py:152
  193.5 14.3 %all-to-all-start.3 = ((bf16[16,12,1024]{2,1,0:T(8,128)(2,1)}), bf16[16,12,1024]{2,1,0:T(8,128)(2,1)S(1)}, u32[]{:S(2)}, u32[]{:S(2)}) async-start(bf16[16,12,1024]{2,1,0:T(8,128)(2,1)} %copy.64), calls=%async_computation.6 | async-start | bytes 1048576 | tf_op jit(solution)/shard_map/all_to_all | solution.py:130
  197.1 11.9 %reduce-scatter.6.cloned.1.call-start = ((), (), s32[]{:S(2)}) async-start(), calls=%async_computation.9 | async-start | bytes 98304 | tf_op jit(solution)/shard_map/reduce_scatter | solution.py:155
Sparse Core Ops, SparseCore 0:
  17.7 24.2 all-reduce.1
  65.0 78.8 reduce-scatter.3
  146.2 4.7 reduce-scatter.7
  199.8 8.7 reduce-scatter.5
where the time goes:
time: 218 us; the launch traced here: 217 us
  waiting for transfers between devices  119 us (55%)
  blocking collectives  37 us (17%)
  starting transfers between devices  17.7 us (8%)
  between operations  14.8 us (7%)
  matrix products  13.6 us (6%)
  local copies, waits for them, and re-layouts  7.75 us (4%)
  other arithmetic  6.66 us (3%)
    reduce_scatter x1, waiting for transfers between devices, shards(): lax.psum_scatter(jnp.dot(features2, paired_weights, preferred_element_typ...  51.5 us
    all_gather x1, blocking collectives, shards(): lax.all_gather(dense_hidden, 'ep', axis=0, tiled=True)  37 us
    psum x1, waiting for transfers between devices, shards(): attn = lax.psum(attn_partial, 'tp').astype(jnp.float32)  23.8 us
    all_to_all x1, waiting for transfers between devices, shards(): lax.all_to_all(send_rows, 'ep', split_axis=0, concat_axis=0, tiled=True)  23.2 us
    all_to_all x1, waiting for transfers between devices, shards(): lax.all_to_all(summed, 'ep', split_axis=0, concat_axis=0, tiled=True)  9.93 us
    all_to_all x1, starting transfers between devices, shards(): lax.all_to_all(normed2, 'ep', split_axis=1, concat_axis=0, tiled=True)  6.83 us
    all_to_all x1, waiting for transfers between devices, shards(): lax.all_to_all(normed2, 'ep', split_axis=1, concat_axis=0, tiled=True)  5.95 us
    all_to_all x1, waiting for transfers between devices, shards(): lax.all_to_all(dense_columns.astype(jnp.bfloat16), 'ep', split_axis=0, co...  5.01 us
  transfers between devices with their start and end apart: 8, of which 6 were waited for; matrix products, arithmetic and copies ran while one was open for 7% of the time, Pallas kernels for 0%

commit v1 on v0

--- a/solution.py
+++ b/solution.py
@@ -132,7 +132,10 @@
     route_rows = returned.reshape(slot_total, half_width)[target]
     route_rows = route_rows.reshape(seq_count, top_count, half_width)
     routed = jnp.sum(gates[:, :, None] * route_rows.astype(jnp.float32), axis=1)
-    features2 = lax.all_to_all(normed2, "ep", split_axis=1, concat_axis=0, tiled=True)
+    features2 = jnp.concatenate(
+        lax.all_to_all(jnp.stack(jnp.split(normed2, lax.axis_size("ep"), axis=1)), "ep", 0, 0),
+        axis=0,
+    )
     paired_weights = jnp.concatenate([w_dense_gate, w_dense_up], axis=1)
     paired = lax.psum_scatter(
         jnp.dot(features2, paired_weights, preferred_element_type=jnp.float32),

time: 218 us -> 226 us (1.037)
  local copies, waits for them, and re-layouts: 7.75 us -> 16.4 us
    unnamed x33 -> x54, local copies, waits for them, and re-layouts: 0.95 us -> 10.4 us
  transfers between devices with their start and end apart: 8 -> 8, of which waited for: 6 -> 6; matrix products, arithmetic and copies ran while one was open for 7% -> 6% of each run, Pallas kernels for 0% -> 0%
where the time goes in v1:
time: 226 us; the launch traced here: 225 us
  waiting for transfers between devices  118 us (52%)
  blocking collectives  37 us (16%)
  starting transfers between devices  17.7 us (8%)
  local copies, waits for them, and re-layouts  16.4 us (7%)
  between operations  14.8 us (7%)
  matrix products  13.7 us (6%)
  other arithmetic  7.17 us (3%)
    reduce_scatter x1, waiting for transfers between devices, shards(): lax.psum_scatter(jnp.dot(features2, paired_weights, preferred_element_typ...  51.4 us
    all_gather x1, blocking collectives, shards(): lax.all_gather(dense_hidden, 'ep', axis=0, tiled=True)  37 us
    all_to_all x1, waiting for transfers between devices, shards(): lax.all_to_all(send_rows, 'ep', split_axis=0, concat_axis=0, tiled=True)  23.2 us
    psum x1, waiting for transfers between devices, shards(): attn = lax.psum(attn_partial, 'tp').astype(jnp.float32)  22.8 us
    unnamed x54, local copies, waits for them, and re-layouts  10.4 us
    all_to_all x1, waiting for transfers between devices, shards(): lax.all_to_all(summed, 'ep', split_axis=0, concat_axis=0, tiled=True)  9.92 us
    all_to_all x1, starting transfers between devices, shards(): lax.all_to_all(jnp.stack(jnp.split(normed2, lax.axis_size('ep'), axis=1))...  6.83 us
    all_to_all x1, waiting for transfers between devices, shards(): lax.all_to_all(jnp.stack(jnp.split(normed2, lax.axis_size('ep'), axis=1))...  5.97 us
  transfers between devices with their start and end apart: 8, of which 6 were waited for; matrix products, arithmetic and copies ran while one was open for 6% of the time, Pallas kernels for 0%

profile of v1, /device:TPU:0, one launch (start us, length us, event | category | flops | bytes accessed | tf_op | source)
XLA Modules:
  0.0 225.4 jit_solution(12497826899775524569)
XLA Ops:
  7.2 1.4 reduce_max.9
  9.3 1.0 fusion.40
  10.3 2.1 convolution_convert_fusion.4
  12.5 3.4 %while.15 = (s32[]{:T(128)}, f32[16,1,8,64]{3,2,0,1:T(8,128)S(1)}, f32[16,1,8]{0,2,1:T(8,128)S(1)}, s32[]{:T(128)}, s32[]{:T(128)}, /*index=5*/s32[16]{0:T(128)S...) while((s32[]{:T(128)}, f32[16,1,8,64]{3,2,0,1:T(8,128)S(1)}, ...), condition=%wide.region_4.5_spmd.clone, body=%wide.region_2.4_spmd.clone.sunk | while | flops 422003200 | bytes 11420495 | solution.py:49
  12.7 1.8 fusion.88
  14.5 0.9 fusion.89
  16.1 1.0 convolution_convert_fusion.2
  18.3 22.8 %all-reduce.2.cloned.1.call-done = bf16[16,2048]{1,0:T(8,128)(2,1)} async-done(((bf16[16,2048]{1,0:T(8,128)(2,1)}), bf16[16,2048]{1,0:T(8,128)(2,1)}) %all-reduce.2.cloned.1.call-update) | async-done | bytes 65552 | tf_op jit(solution)/shard_map/psum | solution.py:100
  41.1 1.0 fusion.37
  42.1 0.7 multiply_reduce_fusion.1
  52.3 6.8 %all-to-all-start = ((bf16[16,16,128]{2,1,0:T(8,128)(2,1)}), bf16[16,16,128]{2,1,0:T(8,128)(2,1)S(1)}, u32[]{:S(2)}, u32[]{:S(2)}) async-start(bf16[16,16,128]{2,1,0:T(8,128)(2,1)} %constant_dynamic-update-slice_fusion), calls=%async_computation | async-start | bytes 131072 | tf_op jit(solution)/shard_map/all_to_all | solution.py:136
  59.5 1.1 reshape.241
  60.7 6.0 %all-to-all-done = bf16[16,16,128]{2,1,0:T(8,128)(2,1)S(1)} async-done(((bf16[16,16,128]{2,1,0:T(8,128)(2,1)}), bf16[16,16,128]{2,1,0:T(8,128)(2,1)S(1)}, u32[]{:S(2)}, u32[]{:S(2)}) %all-to-all-start) | async-done | bytes 65568 | tf_op jit(solution)/shard_map/all_to_all | solution.py:136
  66.7 3.7 %all-to-all-start.2 = ((bf16[16,12,2048]{2,1,0:T(8,128)(2,1)}), bf16[16,12,2048]{2,1,0:T(8,128)(2,1)S(1)}, u32[]{:S(2)}, u32[]{:S(2)}) async-start(bf16[16,12,2048]{2,1,0:T(8,128)(2,1)} %reshape.241), calls=%async_computation.4 | async-start | bytes 2097152 | tf_op jit(solution)/shard_map/all_to_all | solution.py:124
  70.4 1.0 fusion.44
  71.6 23.2 %all-to-all-done.2 = bf16[16,12,2048]{2,1,0:T(8,128)(2,1)S(1)} async-done(((bf16[16,12,2048]{2,1,0:T(8,128)(2,1)}), bf16[16,12,2048]{2,1,0:T(8,128)(2,1)S(1)}, u32[]{:S(2)}, u32[]{:S(2)}) %all-to-all-start.2) | async-done | bytes 786464 | tf_op jit(solution)/shard_map/all_to_all | solution.py:124
  94.8 1.7 convolution_bitcast_fusion.2
  97.0 0.8 copy-done.2
  97.8 1.3 fusion.27
  99.2 0.8 convolution_convert_fusion.6
  100.1 0.8 convolution_convert_fusion.5
  100.9 51.4 %reduce-scatter.4.cloned.1.call-done = f32[16,512]{1,0:T(8,128)} async-done(((f32[256,512]{1,0:T(8,128)}), f32[16,512]{1,0:T(8,128)}) %reduce-scatter.4.cloned.1.call-update) | async-done | bytes 32784 | tf_op jit(solution)/shard_map/reduce_scatter | solution.py:140
  152.3 0.7 fusion.52
  153.1 37.0 %all_gather.3 = bf16[256,256]{1,0:T(8,128)(2,1)S(1)} all-gather(bf16[16,256]{1,0:T(8,128)(2,1)S(1)} %fusion.52), channel_id=1, replica_groups=mesh['ep'=16,'tp'=2] {'ep'}, dimensions={0}, use_global_device_ids=true | all-gather | bytes 139264 | tf_op jit(solution)/shard_map/all_gather | solution.py:151
  190.1 0.8 convolution_convert_fusion.3
  190.9 3.5 %all-to-all-start.1 = ((bf16[16,16,128]{2,1,0:T(8,128)(2,1)}), bf16[16,16,128]{2,1,0:T(8,128)(2,1)S(1)}, u32[]{:S(2)}, u32[]{:S(2)}) async-start(bf16[16,16,128]{2,1,0:T(8,128)(2,1)} %bitcast.20), calls=%async_computation.2 | async-start | bytes 131072 | tf_op jit(solution)/shard_map/all_to_all | solution.py:155
  194.8 2.0 copy.61
  196.8 5.1 %all-to-all-done.1 = bf16[16,16,128]{2,1,0:T(8,128)(2,1)S(1)} async-done(((bf16[16,16,128]{2,1,0:T(8,128)(2,1)}), bf16[16,16,128]{2,1,0:T(8,128)(2,1)S(1)}, u32[]{:S(2)}, u32[]{:S(2)}) %all-to-all-start.1) | async-done | bytes 65568 | tf_op jit(solution)/shard_map/all_to_all | solution.py:155
  201.9 3.6 %all-to-all-start.3 = ((bf16[16,12,1024]{2,1,0:T(8,128)(2,1)}), bf16[16,12,1024]{2,1,0:T(8,128)(2,1)S(1)}, u32[]{:S(2)}, u32[]{:S(2)}) async-start(bf16[16,12,1024]{2,1,0:T(8,128)(2,1)} %copy.61), calls=%async_computation.6 | async-start | bytes 1048576 | tf_op jit(solution)/shard_map/all_to_all | solution.py:130
  206.3 9.9 %all-to-all-done.3 = bf16[16,12,1024]{2,1,0:T(8,128)(2,1)S(1)} async-done(((bf16[16,12,1024]{2,1,0:T(8,128)(2,1)}), bf16[16,12,1024]{2,1,0:T(8,128)(2,1)S(1)}, u32[]{:S(2)}, u32[]{:S(2)}) %all-to-all-start.3) | async-done | bytes 393248 | tf_op jit(solution)/shard_map/all_to_all | solution.py:130
  216.3 0.8 gather_fusion
  217.4 1.5 add_convert_fusion
  (99 shorter events, 14.2 us)
Async XLA Ops:
  7.2 8.9 %copy-start = (bf16[512,2048]{1,0:T(8,128)(2,1)S(1)}, bf16[512,2048]{1,0:T(8,128)(2,1)}, u32[]{:S(2)}) copy-start(bf16[512,2048]{1,0:T(8,128)(2,1)} %param.31) | copy-start | bytes 6291460
  7.2 5.3 %copy-start.8 = (s32[16]{0:T(128)S(1)}, s32[16]{0:T(128)}, u32[]{:S(2)}) copy-start(s32[16]{0:T(128)} %param.23) | copy-start | bytes 196
  7.2 5.3 %copy-start.19 = (f32[8]{0:T(128)S(1)}, f32[8]{0:T(128)}, u32[]{:S(2)}) copy-start(f32[8]{0:T(128)} %param.28) | copy-start | bytes 100
  7.2 33.9 %all-reduce.2.cloned.1.call-start = ((), (), s32[]{:S(2)}) async-start(), calls=%async_computation.7 | async-start | bytes 131072 | tf_op jit(solution)/shard_map/psum | solution.py:100
  12.7 2.7 %copy-start.1 = (bf16[16,1,64,1024]{3,2,0,1:T(8,128)(2,1)S(1)}, bf16[16,1,64,1024]{3,2,0,1:T(8,128)(2,1)}, u32[]{:S(2)}) copy-start(bf16[16,1,64,1024]{3,2,0,1:T(8,128)(2,1)} %get-tuple-element.336) | copy-start | bytes 6291460 | tf_op jit(solution)/shard_map/while
  15.9 1.2 copy-start.7
  15.9 25.2 %copy-start.3 = (bf16[16,2048]{1,0:T(8,128)(2,1)S(1)}, bf16[16,2048]{1,0:T(8,128)(2,1)}, u32[]{:S(2)}) copy-start(bf16[16,2048]{1,0:T(8,128)(2,1)} %param.22) | copy-start | bytes 196612
  15.9 26.2 %copy-start.10 = (f32[2048]{0:T(1024)S(1)}, f32[2048]{0:T(1024)}, u32[]{:S(2)}) copy-start(f32[2048]{0:T(1024)} %param.38) | copy-start | bytes 24580
  16.0 26.1 %copy-start.11 = (f32[2048]{0:T(1024)S(1)}, f32[2048]{0:T(1024)}, u32[]{:S(2)}) copy-start(f32[2048]{0:T(1024)} %param.32) | copy-start | bytes 24580
  17.5 0.5 copy-start.13
  52.3 14.4 %all-to-all-start = ((bf16[16,16,128]{2,1,0:T(8,128)(2,1)}), bf16[16,16,128]{2,1,0:T(8,128)(2,1)S(1)}, u32[]{:S(2)}, u32[]{:S(2)}) async-start(bf16[16,16,128]{2,1,0:T(8,128)(2,1)} %constant_dynamic-update-slice_fusion), calls=%async_computation | async-start | bytes 131072 | tf_op jit(solution)/shard_map/all_to_all | solution.py:136
  59.5 10.9 %copy-start.5 = (bf16[128,256]{1,0:T(8,128)(2,1)S(1)}, bf16[128,256]{1,0:T(8,128)(2,1)}, u32[]{:S(2)}) copy-start(bf16[128,256]{1,0:T(8,128)(2,1)} %param.36) | copy-start | bytes 196612
  59.5 10.9 %copy-start.6 = (bf16[128,256]{1,0:T(8,128)(2,1)S(1)}, bf16[128,256]{1,0:T(8,128)(2,1)}, u32[]{:S(2)}) copy-start(bf16[128,256]{1,0:T(8,128)(2,1)} %param.35) | copy-start | bytes 196612
  66.7 28.1 %all-to-all-start.2 = ((bf16[16,12,2048]{2,1,0:T(8,128)(2,1)}), bf16[16,12,2048]{2,1,0:T(8,128)(2,1)S(1)}, u32[]{:S(2)}, u32[]{:S(2)}) async-start(bf16[16,12,2048]{2,1,0:T(8,128)(2,1)} %reshape.241), calls=%async_computation.4 | async-start | bytes 2097152 | tf_op jit(solution)/shard_map/all_to_all | solution.py:124
  70.3 82.0 %reduce-scatter.4.cloned.1.call-start = ((), (), s32[]{:S(2)}) async-start(), calls=%async_computation.8 | async-start | bytes 557056 | tf_op jit(solution)/shard_map/reduce_scatter | solution.py:140
  71.4 123.3 %reduce-scatter.8.cloned.1.call-start = ((), (), s32[]{:S(2)}) async-start(), calls=%async_computation.10 | async-start | bytes 1179648 | tf_op jit(solution)/shard_map/reduce_scatter | solution.py:63
  94.8 1.8 copy-start.15
  96.6 1.2 copy-start.2
  97.8 1.3 copy-start.14
  97.8 1.4 copy-start.9
  97.8 1.4 copy-start.16
  97.8 2.2 copy-start.17
  97.8 92.2 %copy-start.4 = (bf16[256,128]{1,0:T(8,128)(2,1)S(1)}, bf16[256,128]{1,0:T(8,128)(2,1)}, u32[]{:S(2)}) copy-start(bf16[256,128]{1,0:T(8,128)(2,1)} %param.37) | copy-start | bytes 196612
  97.8 96.5 %copy-start.18 = (bf16[2048,16]{0,1:T(8,128)(2,1)S(1)}, bf16[2048,16]{0,1:T(8,128)(2,1)}, u32[]{:S(2)}) copy-start(bf16[2048,16]{0,1:T(8,128)(2,1)} %param.33) | copy-start | bytes 196612
  99.1 106.5 %copy-start.12 = (f32[16]{0:T(128)S(1)}, f32[16]{0:T(128)}, u32[]{:S(2)}) copy-start(f32[16]{0:T(128)} %get-tuple-element.225) | copy-start | bytes 196
  190.9 11.0 %all-to-all-start.1 = ((bf16[16,16,128]{2,1,0:T(8,128)(2,1)}), bf16[16,16,128]{2,1,0:T(8,128)(2,1)S(1)}, u32[]{:S(2)}, u32[]{:S(2)}) async-start(bf16[16,16,128]{2,1,0:T(8,128)(2,1)} %bitcast.20), calls=%async_computation.2 | async-start | bytes 131072 | tf_op jit(solution)/shard_map/all_to_all | solution.py:155
  201.9 14.3 %all-to-all-start.3 = ((bf16[16,12,1024]{2,1,0:T(8,128)(2,1)}), bf16[16,12,1024]{2,1,0:T(8,128)(2,1)S(1)}, u32[]{:S(2)}, u32[]{:S(2)}) async-start(bf16[16,12,1024]{2,1,0:T(8,128)(2,1)} %copy.61), calls=%async_computation.6 | async-start | bytes 1048576 | tf_op jit(solution)/shard_map/all_to_all | solution.py:130
  205.4 11.9 %reduce-scatter.6.cloned.1.call-start = ((), (), s32[]{:S(2)}) async-start(), calls=%async_computation.9 | async-start | bytes 98304 | tf_op jit(solution)/shard_map/reduce_scatter | solution.py:158
Sparse Core Ops, SparseCore 0:
  17.3 23.7 all-reduce.1
  73.4 78.8 reduce-scatter.3
  154.6 4.7 reduce-scatter.7
  208.1 8.7 reduce-scatter.5
